TPU v7x, 32 devices: a whole 2x2x4 slice. The times are simulated.
32 devices in a mesh: ep: 4 (over y, x), tp: 8 (over z, core).
Axes of the slice: x: 2, y: 2, z: 4, core: 2. Of those that a mesh axis runs over, the one named last changes fastest.
Arguments:
- query_heads_rows: bfloat16 [2048, 2048], P('ep', 'tp'), may hold values from -9 to 9
- key_heads_rows: bfloat16 [2048, 2048], P('ep', 'tp'), may hold values from -9 to 9
- value_heads_rows: bfloat16 [2048, 2048], P('ep', 'tp'), may hold values from -6 to 6
- write_strength_logit: bfloat16 [16, 2048], P('tp', 'ep'), may hold values from -3.5 to -1
- decay_preactivation: bfloat16 [16, 2048], P('tp', 'ep'), may hold values from -5 to 5
- head_decay_logarithm: float32 [16], P('tp'), may hold values from -20 to -3
- extra_log_decay: float32 [16, 2048], P('tp', 'ep'), may hold values from -0.7 to 0
- output_weight: bfloat16 [2048, 2048], P('tp'), may hold values from -2 to 2
- second_batch_tokens: bfloat16 [4096, 2048], P(('ep', 'tp')), may hold values from -6 to 6
- expert_norm_scale: float32 [2048], replicated, may hold values from 0.1 to 1.9
- expert_choice_index: int32 [4096, 2], P(('ep', 'tp')), may hold values from 0 to 15, as said below
- group_router_weight: float32 [4096], P(('ep', 'tp')), may hold values from 0.25 to 1
- expert_logit_difference: float32 [4096], P(('ep', 'tp')), may hold values from -8 to 8
- expert_gate_weight: bfloat16 [16, 1024, 2048], P('ep', 'tp'), may hold values from -0.125 to 0.125
- expert_up_weight: bfloat16 [16, 1024, 2048], P('ep', 'tp'), may hold values from -0.125 to 0.125
- expert_down_weight: bfloat16 [16, 1024, 2048], P('ep', 'tp'), may hold values from -0.375 to 0.375
Outputs:
- mixer_output_first: bfloat16 [2048, 2048], P(('ep', 'tp'))
- expert_out: bfloat16 [4096, 2048], P(('ep', 'tp'))
Inputs may be any that keep to these rules, and one draw needn't show every extreme that they name: `expert_choice_index`: each row names two different experts of one group, the experts a * 4 to a * 4 + 3 for some a. In the rows of one device (aligned blocks of 128 rows) no expert is named more than 32 times, and in every device's rows some expert is named exactly 32 times.
All inputs are finite; a program needn't handle non-finite values.
Results may differ from a plain program's by a relative error of at most 0.018.
Values may be sent and summed in bfloat16 or wider, within the bound.
A program may use at most 128 MiB of HBM per device.

v0:
```python
import jax
import jax.numpy as jnp
from jax import lax
from jax.sharding import PartitionSpec as P

DK = 128
DV = 128
BLOCK = 64
CAP = 32
EXPERTS = 16
TOPK = 2
precise_setting = lax.Precision.HIGHEST
norm_eps = 1e-06


def prefix(value, axis, join, neutral):
    count, mine = (lax.axis_size(axis), lax.axis_index(axis))
    pieces = jax.tree.map(lambda part: lax.all_gather(part, axis), value)
    subtotal = jax.tree.map(
        lambda part, zero: jnp.full_like(part, 0) + jnp.asarray(zero, part.dtype), value, neutral
    )

    def step(position, subtotal):
        longer = join(subtotal, jax.tree.map(lambda part: part[position], pieces))
        return jax.tree.map(lambda new, old: jnp.where(position < mine, new, old), longer, subtotal)

    return lax.fori_loop(0, count - 1, step, subtotal)


def unit_rows(matrix):
    return matrix * lax.rsqrt(jnp.sum(matrix * matrix, axis=-1, keepdims=True) + norm_eps)


def block_terms(query_block, key_block, value_block, decay_logarithm, strength):
    span_len = query_block.shape[2]
    dim_value = value_block.shape[-1]
    cumulative = jnp.cumsum(decay_logarithm, axis=-1)
    within = jnp.tril(jnp.ones((span_len, span_len), bool))
    strict = jnp.tril(jnp.ones((span_len, span_len), bool), -1)
    spread = cumulative[..., :, None] - cumulative[..., None, :]
    decayed = jnp.where(within, jnp.exp(jnp.where(within, spread, 0.0)), 0.0)
    weighted = key_block * strength[..., None]
    lower_part = jnp.where(
        strict,
        jnp.einsum("hnid,hnjd->hnij", weighted, key_block, precision=precise_setting) * decayed,
        0.0,
    )
    system = lower_part + jnp.eye(span_len, dtype=jnp.float32)
    rhs_cols = jnp.concatenate(
        [value_block * strength[..., None], weighted * jnp.exp(cumulative)[..., None]], axis=-1
    )
    solved = jax.scipy.linalg.solve_triangular(system, rhs_cols, lower=True, unit_diagonal=True)
    updated_values = solved[..., :dim_value]
    delta_corrections = solved[..., dim_value:]
    scores = jnp.where(
        within,
        jnp.einsum("hnid,hnjd->hnij", query_block, key_block, precision=precise_setting) * decayed,
        0.0,
    )
    decayed_queries = query_block * jnp.exp(cumulative)[..., None]
    decayed_keys = key_block * jnp.exp(cumulative[..., -1:] - cumulative)[..., None]
    block_retention = jnp.exp(cumulative[..., -1])
    return (
        decayed_queries,
        decayed_keys,
        updated_values,
        delta_corrections,
        scores,
        block_retention,
    )


def carry_step(recurrent_state, inputs):
    decayed_queries, decayed_keys, updated_values, delta_corrections, scores, block_retention = (
        inputs
    )
    value_updates = updated_values - jnp.einsum(
        "jdb,jbu->jdu", delta_corrections, recurrent_state, precision=precise_setting
    )
    final_output = jnp.einsum(
        "jdb,jbu->jdu", decayed_queries, recurrent_state, precision=precise_setting
    )
    final_output = final_output + jnp.einsum(
        "hcj,hjv->hcv", scores, value_updates, precision=precise_setting
    )
    recurrent_state = recurrent_state * block_retention[:, None, None] + jnp.einsum(
        "rpq,rpd->rqd", decayed_keys, value_updates, precision=precise_setting
    )
    return (recurrent_state, final_output)


def compose(earlier, latter):
    joined_map = jnp.einsum("hij,hjk->hik", latter[0], earlier[0], precision=precise_setting)
    joined_state = (
        jnp.einsum("hij,hjv->hiv", latter[0], earlier[1], precision=precise_setting) + latter[1]
    )
    return (joined_map, joined_state)


def shards(
    query_heads_rows,
    key_heads_rows,
    value_heads_rows,
    write_strength_logit,
    decay_preactivation,
    head_decay_logarithm,
    extra_log_decay,
    output_weight,
    second_batch_tokens,
    expert_norm_scale,
    expert_choice_index,
    group_router_weight,
    expert_logit_difference,
    expert_gate_weight,
    expert_up_weight,
    expert_down_weight,
):
    length = query_heads_rows.shape[0]
    local_heads = head_decay_logarithm.shape[0]
    blocks = length // BLOCK
    width_model = output_weight.shape[1]

    def heads_first(matrix):
        spread_out = matrix.astype(jnp.float32).reshape(length, local_heads, -1).transpose(1, 0, 2)
        return spread_out.reshape(local_heads, blocks, BLOCK, -1)

    query_block = unit_rows(heads_first(query_heads_rows)) * DK ** (-0.5)
    key_block = unit_rows(heads_first(key_heads_rows))
    value_block = heads_first(value_heads_rows)
    strength = jax.nn.sigmoid(write_strength_logit.astype(jnp.float32)).reshape(
        local_heads, blocks, BLOCK
    )
    decay_logarithm = (
        -jnp.exp(head_decay_logarithm)[:, None]
        * jax.nn.softplus(decay_preactivation.astype(jnp.float32))
        + extra_log_decay
    )
    decay_logarithm = decay_logarithm.reshape(local_heads, blocks, BLOCK)
    decayed_queries, decayed_keys, updated_values, delta_corrections, scores, block_retention = (
        block_terms(query_block, key_block, value_block, decay_logarithm, strength)
    )
    fresh_wide = jnp.concatenate(
        [updated_values, jnp.zeros(updated_values.shape[:-1] + (DK,), jnp.float32)], axis=-1
    )
    inputs = tuple(
        (
            jnp.moveaxis(term, 1, 0)
            for term in (
                decayed_queries,
                decayed_keys,
                fresh_wide,
                delta_corrections,
                scores,
                block_retention,
            )
        )
    )
    identity_map = jnp.broadcast_to(jnp.eye(DK, dtype=jnp.float32), (local_heads, DK, DK))
    start_memory = jnp.concatenate(
        [jnp.zeros((local_heads, DK, DV), jnp.float32), identity_map], axis=-1
    )
    end_memory, outputs = lax.scan(carry_step, start_memory, inputs)
    local_output = outputs[..., :DV]
    projection_matrix = outputs[..., DV:]
    carried_end = end_memory[..., :DV]
    transfer = end_memory[..., DV:]
    _, incoming_rows = prefix(
        (transfer, carried_end), "ep", compose, (identity_map, jnp.zeros_like(carried_end))
    )
    attention_result = local_output + jnp.einsum(
        "xtyg,tgd->xtyd", projection_matrix, incoming_rows, precision=precise_setting
    )
    attn_rows = (
        attention_result.transpose(0, 2, 1, 3)
        .reshape(length, local_heads * DV)
        .astype(jnp.bfloat16)
    )
    summed = lax.psum_scatter(
        jnp.dot(attn_rows, output_weight, preferred_element_type=jnp.float32).astype(jnp.bfloat16),
        "tp",
        scatter_dimension=0,
        tiled=True,
    )
    widened = second_batch_tokens.astype(jnp.float32)
    normed = (
        widened
        * lax.rsqrt(jnp.mean(widened * widened, axis=-1, keepdims=True) + norm_eps)
        * expert_norm_scale
    ).astype(jnp.bfloat16)
    own_tokens = second_batch_tokens.shape[0]
    ep_count = lax.axis_size("ep")
    local_experts = EXPERTS // ep_count
    flat_ids = expert_choice_index.reshape(-1)
    one_hot = (flat_ids[:, None] == jnp.arange(EXPERTS, dtype=jnp.int32)[None, :]).astype(jnp.int32)
    slot_rank = jnp.sum((jnp.cumsum(one_hot, axis=0) - one_hot) * one_hot, axis=1)
    slot_index = flat_ids * CAP + slot_rank
    copy_token = jnp.arange(flat_ids.shape[0], dtype=jnp.int32) // TOPK
    slot_token = jnp.full((EXPERTS * CAP,), own_tokens, jnp.int32).at[slot_index].set(copy_token)
    outgoing = jnp.take(normed, slot_token, axis=0, mode="fill", fill_value=0).reshape(
        ep_count, local_experts, CAP, width_model
    )
    arrived = lax.all_to_all(outgoing, "ep", split_axis=0, concat_axis=0, tiled=True)
    gate_piece = lax.all_gather(expert_gate_weight, "tp", axis=1, tiled=True)
    up_piece = lax.all_gather(expert_up_weight, "tp", axis=1, tiled=True)
    down_piece = lax.all_gather(expert_down_weight, "tp", axis=1, tiled=True)
    gating = jnp.einsum("secd,efd->secf", arrived, gate_piece, preferred_element_type=jnp.float32)
    upward = jnp.einsum("secd,efd->secf", arrived, up_piece, preferred_element_type=jnp.float32)
    hidden = (jax.nn.silu(gating) * upward).astype(jnp.bfloat16)
    produced = jnp.einsum("secf,efd->secd", hidden, down_piece, preferred_element_type=jnp.float32)
    returned = lax.all_to_all(
        produced.astype(jnp.bfloat16), "ep", split_axis=0, concat_axis=0, tiled=True
    )
    flat_results = returned.reshape(EXPERTS * CAP, width_model)
    picked = (
        jnp.take(flat_results, slot_index, axis=0)
        .reshape(own_tokens, TOPK, width_model)
        .astype(jnp.float32)
    )
    leading = jax.nn.sigmoid(expert_logit_difference)
    mixing = group_router_weight[:, None] * jnp.stack([leading, 1.0 - leading], axis=-1)
    expert_out = jnp.sum(mixing[..., None] * picked, axis=1).astype(jnp.bfloat16)
    return (summed, expert_out)


def solution(mesh):
    in_specs = (
        P("ep", "tp"),
        P("ep", "tp"),
        P("ep", "tp"),
        P("tp", "ep"),
        P("tp", "ep"),
        P("tp"),
        P("tp", "ep"),
        P("tp", None),
        P(("ep", "tp"), None),
        P(),
        P(("ep", "tp"), None),
        P(("ep", "tp")),
        P(("ep", "tp")),
        P("ep", "tp", None),
        P("ep", "tp", None),
        P("ep", "tp", None),
    )
    out_specs = (P(("ep", "tp"), None), P(("ep", "tp"), None))
    return jax.shard_map(shards, mesh=mesh, in_specs=in_specs, out_specs=out_specs, check_vma=False)
```

profile of v0, /device:TPU:0, one launch (start us, length us, event | category | flops | bytes accessed | tf_op | source)
XLA Modules:
  0.0 520.2 jit_solution(1640668718798541853)
XLA Ops:
  11.6 1.4 scatter_custom_fusion
  13.5 3.3 gather_fusion
  16.9 3.1 broadcast_select_fusion
  20.0 5.6 %all-to-all-start = ((bf16[4,4,32,2048]{3,2,1,0:T(8,128)(2,1)}), bf16[4,4,32,2048]{3,2,1,0:T(8,128)(2,1)S(1)}, u32[]{:S(2)}, u32[]{:S(2)}) async-start(bf16[4,4,32,2048]{3,2,1,0:T(8,128)(2,1)} %broadcast_select_fusion), calls=%async_computation.1 | async-start | bytes 4194304 | tf_op jit(solution)/shard_map/all_to_all | solution.py:202
  29.5 3.0 fusion.52
  32.4 80.0 %custom-call.4 = f32[2,8,1,64,64]{3,4,2,1,0:T(8,128)} custom-call(f32[2,8,1,64,64]{4,3,2,1,0:T(8,128)} %fusion.52), custom_call_target="InvertDiagBlocksLowerTriangular" | custom-call | tf_op jit(solution)/shard_map/jit(_solve_triangular)/vmap(vmap())/triangular_solve | solution.py:52
  114.4 2.0 copy.100
  119.9 2.5 multiply_multiply_fusion
  125.6 2.0 fusion.50
  128.6 48.9 %while.26 = (s32[]{:T(128)}, f32[2,128,256]{2,1,0:T(8,128)S(1)}, f32[8,2,64,256]{3,2,0,1:T(8,128)}, f32[8,2]{1,0:T(8,128)}, f32[8,2,64,128]{3,2,0,1:T(8,128)}, /...) while((s32[]{:T(128)}, f32[2,128,256]{2,1,0:T(8,128)S(1)}, ...), condition=%wide.region_4.5_spmd, body=%wide.region_3.4_spmd.sunk | while | flops 176357376 | bytes 2231425 | solution.py:162
  128.6 1.2 convolution_subtract_fusion.2
  131.0 1.8 fusion.127
  133.5 1.3 convolution_add_fusion.4
  137.1 1.8 fusion.127
  139.6 1.3 convolution_add_fusion.4
  143.2 1.8 fusion.127
  145.7 1.3 convolution_add_fusion.4
  149.3 1.8 fusion.127
  151.8 1.3 convolution_add_fusion.4
  155.4 1.8 fusion.127
  157.9 1.3 convolution_add_fusion.4
  161.5 1.8 fusion.127
  164.0 1.3 convolution_add_fusion.4
  165.2 1.2 convolution_subtract_fusion.2
  167.6 1.8 fusion.127
  170.1 1.3 convolution_add_fusion.4
  171.4 1.3 convolution_subtract_fusion.2
  173.8 1.8 fusion.127
  176.3 1.3 convolution_add_fusion.4
  177.6 11.2 %all-gather = f32[8,128,128]{2,1,0:T(8,128)} all-gather(f32[2,128,128]{2,1,0:T(8,128)S(1)} %get-tuple-element.243), channel_id=2, replica_groups=mesh['ep'=4,'tp'=8] {'ep'}, dimensions={0}, use_global_device_ids=true | all-gather | bytes 655360 | tf_op jit(solution)/shard_map/all_gather | solution.py:18
  188.8 11.2 %all-gather.1 = f32[8,128,128]{2,1,0:T(8,128)} all-gather(f32[2,128,128]{2,1,0:T(8,128)S(1)} %get-tuple-element.242), channel_id=3, replica_groups=mesh['ep'=4,'tp'=8] {'ep'}, dimensions={0}, use_global_device_ids=true | all-gather | bytes 655360 | tf_op jit(solution)/shard_map/all_gather | solution.py:18
  200.1 4.0 while.27
  200.1 1.2 fusion.130
  201.4 1.2 fusion.130
  202.7 1.2 fusion.130
  204.1 1.8 fusion.55
  206.2 2.1 convolution_convert_fusion
  208.4 12.9 %fusion.26 = f32[4,4,32,1024]{3,2,1,0:T(8,128)} fusion(bf16[4,1024,2048]{2,1,0:T(8,128)(2,1)} %all-gather.8.cloned.1.call-done, bf16[4,4,32,2048]{3,2,1,0:T(8,128)(2,1)S(1)} %all-to-all-done), kind=kOutput, calls=%fused_computation.34 | convolution fusion | flops 2147483648 | bytes 20971520 | tf_op jit(solution)/shard_map/secd,efd->secf/dot_general | solution.py:207
  221.3 93.1 %all-gather.6.cloned.1.call-done = bf16[4,1024,2048]{2,1,0:T(8,128)(2,1)} async-done(((bf16[4,128,2048]{2,1,0:T(8,128)(2,1)}), bf16[4,1024,2048]{2,1,0:T(8,128)(2,1)}) %all-gather.6.cloned.1.call-update) | async-done | bytes 16777232 | tf_op jit(solution)/shard_map/all_gather | solution.py:203
  314.3 13.1 %fusion.36 = bf16[4,4,32,1024]{3,2,0,1:T(8,128)(2,1)} fusion(f32[4,4,32,1024]{3,2,1,0:T(8,128)} %fusion.26, bf16[4,1024,2048]{2,1,0:T(8,128)(2,1)} %all-gather.6.cloned.1.call-done, bf16[4,4,32,2048]{3,2,1,0:T(8,128)(2,1)S(1)} %all-to-all-done), kind=kOutput, calls=%fused_computation.42 | convolution fusion | flops 2150629376 | bytes 22020096 | tf_op jit(solution)/shard_map/secd,efd->secf/dot_general | solution.py:206
  327.4 137.8 %all-gather.10.cloned.1.call-done = bf16[4,1024,2048]{2,1,0:T(8,128)(2,1)} async-done(((bf16[4,128,2048]{2,1,0:T(8,128)(2,1)}), bf16[4,1024,2048]{2,1,0:T(8,128)(2,1)}) %all-gather.10.cloned.1.call-update) | async-done | bytes 16777232 | tf_op jit(solution)/shard_map/all_gather | solution.py:205
  465.3 8.5 %fusion.33 = bf16[4,4,32,2048]{3,2,0,1:T(8,128)(2,1)S(1)} fusion(bf16[4,4,32,1024]{3,2,0,1:T(8,128)(2,1)} %fusion.36, bf16[4,1024,2048]{2,1,0:T(8,128)(2,1)} %all-gather.10.cloned.1.call-done), kind=kOutput, calls=%fused_computation.40 | convolution fusion | flops 2148532224 | bytes 19922944 | tf_op jit(solution)/shard_map/secf,efd->secd/dot_general | solution.py:209
  473.7 1.6 copy.119
  475.3 4.0 all-to-all-start.1
  479.9 24.7 %all-to-all-done.1 = bf16[4,4,32,2048]{3,2,1,0:T(8,128)(2,1)S(1)} async-done(((bf16[4,4,32,2048]{3,2,1,0:T(8,128)(2,1)}), bf16[4,4,32,2048]{3,2,1,0:T(8,128)(2,1)S(1)}, u32[]{:S(2)}, u32[]{:S(2)}) %all-to-all-start.1) | async-done | bytes 2097184 | tf_op jit(solution)/shard_map/all_to_all | solution.py:210
  504.6 2.3 gather_fusion.1
  507.0 1.7 gather.15
  508.7 4.9 multiply_reduce_fusion
  (148 shorter events, 39.8 us)
Async XLA Ops:
  7.2 199.1 %copy-start = (bf16[256,2048]{1,0:T(8,128)(2,1)S(1)}, bf16[256,2048]{1,0:T(8,128)(2,1)}, u32[]{:S(2)}) copy-start(bf16[256,2048]{1,0:T(8,128)(2,1)} %param.27) | copy-start | bytes 3145732
  7.2 201.2 %all-gather.8.cloned.1.call-start = ((), (), s32[]{:S(2)}) async-start(), calls=%async_computation.5 | async-start | bytes 18874368 | tf_op jit(solution)/shard_map/all_gather | solution.py:204
  7.9 1.5 copy-start.11
  7.9 5.2 %copy-start.2 = (bf16[128,2048]{1,0:T(8,128)(2,1)S(1)}, bf16[128,2048]{1,0:T(8,128)(2,1)}, u32[]{:S(2)}) copy-start(bf16[128,2048]{1,0:T(8,128)(2,1)} %param.28) | copy-start | bytes 1572868
  7.9 5.4 %copy-start.14 = (f32[2048]{0:T(1024)S(1)}, f32[2048]{0:T(1024)}, u32[]{:S(2)}) copy-start(f32[2048]{0:T(1024)} %param.29) | copy-start | bytes 24580
  7.9 306.4 %all-gather.6.cloned.1.call-start = ((), (), s32[]{:S(2)}) async-start(), calls=%async_computation.4 | async-start | bytes 18874368 | tf_op jit(solution)/shard_map/all_gather | solution.py:203
  8.7 456.6 %all-gather.10.cloned.1.call-start = ((), (), s32[]{:S(2)}) async-start(), calls=%async_computation.6 | async-start | bytes 18874368 | tf_op jit(solution)/shard_map/all_gather | solution.py:205
  11.0 0.6 copy-start.9
  11.6 1.5 copy-start.17
  20.0 5.6 %copy-start.23 = (f32[2]{0:T(128)S(1)}, f32[2]{0:T(128)}, u32[]{:S(2)}) copy-start(f32[2]{0:T(128)} %param.25) | copy-start | bytes 28
  20.0 5.6 %copy-start.19 = (f32[2,512]{1,0:T(2,128)S(1)}, f32[2,512]{1,0:T(2,128)}, u32[]{:S(2)}) copy-start(f32[2,512]{1,0:T(2,128)} %param.26) | copy-start | bytes 12292
  20.0 5.6 %copy-start.20 = (bf16[2,512]{1,0:T(2,128)(2,1)S(1)}, bf16[2,512]{1,0:T(2,128)(2,1)}, u32[]{:S(2)}) copy-start(bf16[2,512]{1,0:T(2,128)(2,1)} %param.24) | copy-start | bytes 6148
  20.0 5.8 %copy-start.6 = (bf16[512,256]{1,0:T(8,128)(2,1)S(1)}, bf16[512,256]{1,0:T(8,128)(2,1)}, u32[]{:S(2)}) copy-start(bf16[512,256]{1,0:T(8,128)(2,1)} %param.21) | copy-start | bytes 786436
  20.0 188.4 %all-to-all-start = ((bf16[4,4,32,2048]{3,2,1,0:T(8,128)(2,1)}), bf16[4,4,32,2048]{3,2,1,0:T(8,128)(2,1)S(1)}, u32[]{:S(2)}, u32[]{:S(2)}) async-start(bf16[4,4,32,2048]{3,2,1,0:T(8,128)(2,1)} %broadcast_select_fusion), calls=%async_computation.1 | async-start | bytes 4194304 | tf_op jit(solution)/shard_map/all_to_all | solution.py:202
  25.6 488.0 %reduce-scatter.2.cloned.1.call-start = ((), (), s32[]{:S(2)}) async-start(), calls=%async_computation.3 | async-start | bytes 2359296 | tf_op jit(solution)/shard_map/reduce_scatter | solution.py:178
  28.6 0.6 copy-start.15
  28.7 0.8 copy-start.4
  116.8 0.6 copy-start.13
  118.1 4.3 copy-start.7
  122.4 2.0 copy-start.3
  122.4 3.1 copy-start.5
  122.4 3.1 copy-start.8
  122.4 3.1 copy-start.16
  123.6 4.0 copy-start.21
  475.3 4.0 copy-start.10
  475.3 4.2 copy-start.12
  475.3 4.4 copy-start.24
  475.3 4.4 copy-start.22
  475.3 4.6 copy-start.18
  475.3 29.3 %all-to-all-start.1 = ((bf16[4,4,32,2048]{3,2,1,0:T(8,128)(2,1)}), bf16[4,4,32,2048]{3,2,1,0:T(8,128)(2,1)S(1)}, u32[]{:S(2)}, u32[]{:S(2)}) async-start(bf16[4,4,32,2048]{3,2,1,0:T(8,128)(2,1)} %copy.119), calls=%async_computation.2 | async-start | bytes 4194304 | tf_op jit(solution)/shard_map/all_to_all | solution.py:210
  504.6 9.0 %copy-start.1 = (bf16[256,2048]{1,0:T(8,128)(2,1)S(1)}, bf16[256,2048]{1,0:T(8,128)(2,1)}, u32[]{:S(2)}) copy-start(bf16[256,2048]{1,0:T(8,128)(2,1)} %param.27) | copy-start | bytes 3145732
Sparse Core Ops, SparseCore 0:
  9.6 153.7 all-gather.7
  165.0 149.2 all-gather.5
  316.0 149.2 all-gather.9
  468.0 34.1 reduce-scatter.1
where the time goes:
time: 522 us; the launch traced here: 520 us
  waiting for transfers between devices  258 us (49%)
  other arithmetic  98.3 us (19%)
  matrix products  91.2 us (17%)
  local copies, waits for them, and re-layouts  26 us (5%)
  blocking collectives  22.5 us (4%)
  between operations  14.2 us (3%)
  starting transfers between devices  9.7 us (2%)
    all_gather x1, waiting for transfers between devices, shards(): down_piece = lax.all_gather(expert_down_weight, 'tp', axis=1, tiled=True)  138 us
    all_gather x1, waiting for transfers between devices, shards(): gate_piece = lax.all_gather(expert_gate_weight, 'tp', axis=1, tiled=True)  93.1 us
    another operation x2, other arithmetic, block_terms(): jax.scipy.linalg.solve_triangular(system, rhs_cols, lower=True, unit_diag...  80 us
    all_to_all x1, waiting for transfers between devices, shards(): lax.all_to_all(produced.astype(jnp.bfloat16), 'ep', split_axis=0, concat_...  24.7 us
    all_gather x2, blocking collectives, prefix(): pieces = jax.tree.map(lambda part: lax.all_gather(part, axis), value)  22.5 us
    dot_general x8, matrix products, carry_step(): jnp.einsum('hcj,hjv->hcv', scores, value_updates, precision=precise_setting)  14.2 us
    dot_general x1, matrix products, shards(): jnp.einsum('secd,efd->secf', arrived, gate_piece, preferred_element_type=...  13.1 us
    dot_general x1, matrix products, shards(): jnp.einsum('secd,efd->secf', arrived, up_piece, preferred_element_type=jn...  12.9 us
  transfers between devices with their start and end apart: 6, of which 3 were waited for; matrix products, arithmetic and copies ran while one was open for 41% of the time, Pallas kernels for 0%

commit v1 on v0

--- a/solution.py
+++ b/solution.py
@@ -11,6 +11,28 @@
 TOPK = 2
 precise_setting = lax.Precision.HIGHEST
 norm_eps = 1e-06
+
+
+def _check_cubes(incoming_x, axis_tag, d0, u):
+    local_out, n_now, built = (
+        lax.axis_size(axis_tag),
+        lax.axis_index(axis_tag),
+        incoming_x.shape[d0],
+    )
+    block_list = [(ii, (ii + 1) % local_out) for ii in range(local_out)]
+    windows = [(ii, (ii - 1) % local_out) for ii in range(local_out)]
+    r_now = local_out // 2
+    t1 = work_now = incoming_x
+    item_now = u(incoming_x, n_now * built)
+    p = 1
+    while p < r_now + 1:
+        t1 = lax.ppermute(t1, axis_tag, block_list)
+        if p < local_out - r_now:
+            work_now = lax.ppermute(work_now, axis_tag, windows)
+            item_now = item_now + u(work_now, (n_now + p) % local_out * built)
+        item_now = item_now + u(t1, (n_now - p) % local_out * built)
+        p += 1
+    return item_now
 
 
 def prefix(value, axis, join, neutral):
@@ -202,11 +224,20 @@
     arrived = lax.all_to_all(outgoing, "ep", split_axis=0, concat_axis=0, tiled=True)
     gate_piece = lax.all_gather(expert_gate_weight, "tp", axis=1, tiled=True)
     up_piece = lax.all_gather(expert_up_weight, "tp", axis=1, tiled=True)
-    down_piece = lax.all_gather(expert_down_weight, "tp", axis=1, tiled=True)
     gating = jnp.einsum("secd,efd->secf", arrived, gate_piece, preferred_element_type=jnp.float32)
     upward = jnp.einsum("secd,efd->secf", arrived, up_piece, preferred_element_type=jnp.float32)
     hidden = (jax.nn.silu(gating) * upward).astype(jnp.bfloat16)
-    produced = jnp.einsum("secf,efd->secd", hidden, down_piece, preferred_element_type=jnp.float32)
+    produced = _check_cubes(
+        expert_down_weight,
+        "tp",
+        1,
+        lambda shard, offset: jnp.einsum(
+            "secf,efd->secd",
+            lax.dynamic_slice_in_dim(hidden, offset, shard.shape[1], axis=3),
+            shard,
+            preferred_element_type=jnp.float32,
+        ),
+    )
     returned = lax.all_to_all(
         produced.astype(jnp.bfloat16), "ep", split_axis=0, concat_axis=0, tiled=True
     )

time: 522 us -> 546 us (1.046)
  starting transfers between devices: 9.7 us -> 54.3 us
  waiting for transfers between devices: 258 us -> 222 us
  matrix products: 91.2 us -> 112 us
  local copies, waits for them, and re-layouts: 26 us -> 19 us
    all_gather x1 -> x0, waiting for transfers between devices: 138 us -> none  [shards(): down_piece = lax.all_gather(expert_down_weight, 'tp', axis=1, tiled=True)]
    ppermute x0 -> x7, waiting for transfers between devices: none -> 53.4 us  [the longest x4 53.4 us: _check_cubes(): t1 = lax.ppermute(t1, axis_tag, block_list)]
    all_gather x1, waiting for transfers between devices: 93.1 us -> 142 us  [shards(): gate_piece = lax.all_gather(expert_gate_weight, 'tp', axis=1, tiled=True)]
    ppermute x0 -> x7, starting transfers between devices: none -> 46.2 us  [the longest x3 45 us: _check_cubes(): work_now = lax.ppermute(work_now, axis_tag, windows)]
    dot_general x1 -> x8, matrix products: 8.46 us -> 31.4 us  [shards(): jnp.einsum('secf,efd->secd', lax.dynamic_slice_in_dim(hidden, offset, sha...]
    mul x8, local copies, waits for them, and re-layouts: 5.52 us -> 0.04 us  [carry_step(): recurrent_state * block_retention[:, None, None]]
  transfers between devices with their start and end apart: 6 -> 12, of which waited for: 3 -> 3; matrix products, arithmetic and copies ran while one was open for 41% -> 42% of each run, Pallas kernels for 0% -> 0%
where the time goes in v1:
time: 546 us; the launch traced here: 543 us
  waiting for transfers between devices  222 us (41%)
  matrix products  112 us (21%)
  other arithmetic  98.2 us (18%)
  starting transfers between devices  54.3 us (10%)
  blocking collectives  23.6 us (4%)
  local copies, waits for them, and re-layouts  19 us (3%)
  between operations  14.3 us (3%)
    all_gather x1, waiting for transfers between devices, shards(): gate_piece = lax.all_gather(expert_gate_weight, 'tp', axis=1, tiled=True)  142 us
    another operation x2, other arithmetic, block_terms(): jax.scipy.linalg.solve_triangular(system, rhs_cols, lower=True, unit_diag...  80 us
    ppermute x4, waiting for transfers between devices, _check_cubes(): t1 = lax.ppermute(t1, axis_tag, block_list)  53.4 us
    ppermute x3, starting transfers between devices, _check_cubes(): work_now = lax.ppermute(work_now, axis_tag, windows)  45 us
    dot_general x8, matrix products, shards(): jnp.einsum('secf,efd->secd', lax.dynamic_slice_in_dim(hidden, offset, sha...  31.4 us
    all_to_all x1, waiting for transfers between devices, shards(): lax.all_to_all(produced.astype(jnp.bfloat16), 'ep', split_axis=0, concat_...  24.9 us
    all_gather x2, blocking collectives, prefix(): pieces = jax.tree.map(lambda part: lax.all_gather(part, axis), value)  23.6 us
    dot_general x8, matrix products, carry_step(): jnp.einsum('hcj,hjv->hcv', scores, value_updates, precision=precise_setting)  14.1 us
  transfers between devices with their start and end apart: 12, of which 3 were waited for; matrix products, arithmetic and copies ran while one was open for 42% of the time, Pallas kernels for 0%

profile of v1, /device:TPU:0, one launch (start us, length us, event | category | flops | bytes accessed | tf_op | source)
XLA Modules:
  0.0 543.4 jit_solution(2958217090373059836)
XLA Ops:
  9.2 4.1 collective-permute-start
  14.9 1.4 scatter_custom_fusion
  16.9 3.3 gather_fusion
  20.1 3.4 broadcast_select_fusion
  23.6 4.3 all-to-all-start
  31.4 2.2 fusion.60
  34.5 53.4 %collective-permute-done.1 = bf16[4,128,2048]{2,1,0:T(8,128)(2,1)} collective-permute-done((bf16[4,128,2048]{2,1,0:T(8,128)(2,1)}, bf16[4,128,2048]{2,1,0:T(8,128)(2,1)}, u32[]{:S(2)}, u32[]{:S(2)}) %collective-permute-start.1) | collective-permute-done | bytes 2097184 | tf_op jit(solution)/shard_map/ppermute | solution.py:29
  88.6 80.0 %custom-call.4 = f32[2,8,1,64,64]{3,4,2,1,0:T(8,128)} custom-call(f32[2,8,1,64,64]{4,3,2,1,0:T(8,128)} %fusion.60), custom_call_target="InvertDiagBlocksLowerTriangular" | custom-call | tf_op jit(solution)/shard_map/jit(_solve_triangular)/vmap(vmap())/triangular_solve | solution.py:74
  168.6 2.1 copy.100
  172.0 2.5 multiply_multiply_fusion
  177.6 2.0 fusion.58
  180.6 2.8 collective-permute-start.2
  183.5 43.3 %while.26 = (s32[]{:T(128)}, f32[2,128,256]{2,1,0:T(8,128)S(1)}, f32[8,2,64,256]{3,2,0,1:T(8,128)}, f32[8,2]{1,0:T(8,128)S(1)}, f32[8,2,64,128]{3,2,0,1:T(8,128)...) while((s32[]{:T(128)}, f32[2,128,256]{2,1,0:T(8,128)S(1)}, ...), condition=%wide.region_4.5_spmd, body=%wide.region_3.4_spmd.sunk | while | flops 176357376 | bytes 2231425 | solution.py:184
  185.8 1.8 fusion.150
  187.6 1.3 convolution_add_fusion.4
  191.2 1.8 fusion.150
  193.0 1.3 convolution_add_fusion.4
  196.7 1.8 fusion.150
  202.1 1.8 fusion.150
  207.5 1.8 fusion.150
  209.3 1.3 convolution_add_fusion.4
  212.9 1.8 fusion.150
  218.4 1.8 fusion.150
  223.8 1.8 fusion.150
  227.5 13.8 %all-gather = f32[8,128,128]{2,1,0:T(8,128)} all-gather(f32[2,128,128]{2,1,0:T(8,128)} %get-tuple-element.243), channel_id=2, replica_groups=mesh['ep'=4,'tp'=8] {'ep'}, dimensions={0}, use_global_device_ids=true | all-gather | bytes 655360 | tf_op jit(solution)/shard_map/all_gather | solution.py:40
  241.3 9.8 %all-gather.1 = f32[8,128,128]{2,1,0:T(8,128)} all-gather(f32[2,128,128]{2,1,0:T(8,128)S(1)} %get-tuple-element.242), channel_id=3, replica_groups=mesh['ep'=4,'tp'=8] {'ep'}, dimensions={0}, use_global_device_ids=true | all-gather | bytes 655360 | tf_op jit(solution)/shard_map/all_gather | solution.py:40
  251.1 3.9 while.27
  251.1 1.3 fusion.153
  255.0 1.8 fusion.63
  257.0 2.1 convolution_convert_fusion
  259.3 38.0 %collective-permute-start.4 = (bf16[4,128,2048]{2,1,0:T(8,128)(2,1)}, bf16[4,128,2048]{2,1,0:T(8,128)(2,1)}, u32[]{:S(2)}, u32[]{:S(2)}) collective-permute-start(bf16[4,128,2048]{2,1,0:T(8,128)(2,1)} %collective-permute-done.2), channel_id=1, source_target_pairs={{0,7},{1,0},{2,1},{3,2},{4,3},{5,4},{6,5},{7,6},{8,15},{9,8},{10,9... | collective-permute-start | bytes 6291464 | tf_op jit(solution)/shard_map/ppermute | solution.py:31
  297.4 12.7 %fusion.24 = f32[4,4,32,1024]{3,2,1,0:T(8,128)} fusion(bf16[4,1024,2048]{2,1,0:T(8,128)(2,1)} %all-gather.7.cloned.1.call-done, bf16[4,4,32,2048]{3,2,1,0:T(8,128)(2,1)S(1)} %all-to-all-done), kind=kOutput, calls=%fused_computation.32 | convolution fusion | flops 2147483648 | bytes 20971520 | tf_op jit(solution)/shard_map/secd,efd->secf/dot_general | solution.py:228
  310.1 141.9 %all-gather.5.cloned.1.call-done = bf16[4,1024,2048]{2,1,0:T(8,128)(2,1)} async-done(((bf16[4,128,2048]{2,1,0:T(8,128)(2,1)}), bf16[4,1024,2048]{2,1,0:T(8,128)(2,1)}) %all-gather.5.cloned.1.call-update) | async-done | bytes 16777232 | tf_op jit(solution)/shard_map/all_gather | solution.py:225
  452.0 12.1 %fusion.44 = bf16[4,4,32,1024]{3,2,0,1:T(8,128)(2,1)S(1)} fusion(f32[4,4,32,1024]{3,2,1,0:T(8,128)} %fusion.24, bf16[4,1024,2048]{2,1,0:T(8,128)(2,1)} %all-gather.5.cloned.1.call-done, bf16[4,4,32,2048]{3,2,1,0:T(8,128)(2,1)S(1)} %all-to-all-done), kind=kOutput, calls=%fused_computation.55 | convolution fusion | flops 2150629376 | bytes 22020096 | tf_op jit(solution)/shard_map/secd,efd->secf/dot_general | solution.py:227
  464.0 2.3 fusion.42
  466.3 2.3 fusion.30
  468.6 2.3 fusion.34
  471.0 2.3 fusion.36
  473.3 4.3 fusion.38
  477.5 4.3 fusion.40
  481.8 4.5 fusion.32
  486.4 9.1 %fusion.28 = bf16[4,4,32,2048]{3,2,0,1:T(8,128)(2,1)} fusion(f32[4,4,32,2048]{3,2,1,0:T(8,128)S(1)} %fusion.30, f32[4,4,32,2048]{3,2,1,0:T(8,128)} %fusion.32, f32[4,4,32,2048]{3,2,1,0:T(8,128)S(1)} %fusion.34, f32[4,4,32,2048]{3,2,1,0:T(8,128)S(1)} %fusion.36, f32[4,4,32,2048]{3,2,1,0:T(8,128)} %fusion.38, f32[4,4,32,2048]{3,2,1,0:T(8,128)S(1)} %fusion.42, ...), kind=kOutput, calls=%fused_computation.38 | convolution fusion | flops 276824064 | bytes 33685508 | tf_op jit(solution)/shard_map/secf,efd->secd/dot_general | solution.py:234
  495.5 3.2 copy.119
  498.7 3.7 all-to-all-start.1
  503.0 24.9 %all-to-all-done.1 = bf16[4,4,32,2048]{3,2,1,0:T(8,128)(2,1)S(1)} async-done(((bf16[4,4,32,2048]{3,2,1,0:T(8,128)(2,1)}), bf16[4,4,32,2048]{3,2,1,0:T(8,128)(2,1)S(1)}, u32[]{:S(2)}, u32[]{:S(2)}) %all-to-all-start.1) | async-done | bytes 2097184 | tf_op jit(solution)/shard_map/all_to_all | solution.py:241
  527.9 2.3 gather_fusion.1
  530.2 1.7 gather.15
  532.0 4.9 multiply_reduce_fusion
  (150 shorter events, 43.8 us)
Async XLA Ops:
  7.2 249.9 %copy-start = (bf16[256,2048]{1,0:T(8,128)(2,1)S(1)}, bf16[256,2048]{1,0:T(8,128)(2,1)}, u32[]{:S(2)}) copy-start(bf16[256,2048]{1,0:T(8,128)(2,1)} %param.27) | copy-start | bytes 3145732
  7.2 6.2 %copy-start.8 = (s32[128,2]{0,1:T(2,128)S(1)}, s32[128,2]{0,1:T(2,128)}, u32[]{:S(2)}) copy-start(s32[128,2]{0,1:T(2,128)} %param.30) | copy-start | bytes 3076
  7.2 9.3 %copy-start.2 = (bf16[128,2048]{1,0:T(8,128)(2,1)S(1)}, bf16[128,2048]{1,0:T(8,128)(2,1)}, u32[]{:S(2)}) copy-start(bf16[128,2048]{1,0:T(8,128)(2,1)} %param.28) | copy-start | bytes 1572868
  7.2 9.5 %copy-start.9 = (f32[2048]{0:T(1024)S(1)}, f32[2048]{0:T(1024)}, u32[]{:S(2)}) copy-start(f32[2048]{0:T(1024)} %param.29) | copy-start | bytes 24580
  7.2 290.1 %all-gather.7.cloned.1.call-start = ((), (), s32[]{:S(2)}) async-start(), calls=%async_computation.5 | async-start | bytes 18874368 | tf_op jit(solution)/shard_map/all_gather | solution.py:226
  7.9 444.0 %all-gather.5.cloned.1.call-start = ((), (), s32[]{:S(2)}) async-start(), calls=%async_computation.4 | async-start | bytes 18874368 | tf_op jit(solution)/shard_map/all_gather | solution.py:225
  8.7 79.2 %collective-permute-start.1 = (bf16[4,128,2048]{2,1,0:T(8,128)(2,1)}, bf16[4,128,2048]{2,1,0:T(8,128)(2,1)}, u32[]{:S(2)}, u32[]{:S(2)}) collective-permute-start(bf16[4,128,2048]{2,1,0:T(8,128)(2,1)} %param.35), channel_id=1, source_target_pairs={{0,1},{1,2},{2,3},{3,4},{4,5},{5,6},{6,7},{7,0},{8,9},{9,10},{10,1... | collective-permute-start | bytes 6291464 | tf_op jit(solution)/shard_map/ppermute | solution.py:29
  9.2 171.4 %collective-permute-start = (bf16[4,128,2048]{2,1,0:T(8,128)(2,1)}, bf16[4,128,2048]{2,1,0:T(8,128)(2,1)}, u32[]{:S(2)}, u32[]{:S(2)}) collective-permute-start(bf16[4,128,2048]{2,1,0:T(8,128)(2,1)} %param.35), channel_id=1, source_target_pairs={{0,7},{1,0},{2,1},{3,2},{4,3},{5,4},{6,5},{7,6},{8,15},{9,8},{10,9... | collective-permute-start | bytes 6291464 | tf_op jit(solution)/shard_map/ppermute | solution.py:31
  23.6 4.3 copy-start.6
  23.6 4.6 copy-start.15
  23.6 4.6 copy-start.10
  23.6 4.6 copy-start.12
  23.6 4.8 copy-start.11
  23.6 273.7 %all-to-all-start = ((bf16[4,4,32,2048]{3,2,1,0:T(8,128)(2,1)}), bf16[4,4,32,2048]{3,2,1,0:T(8,128)(2,1)S(1)}, u32[]{:S(2)}, u32[]{:S(2)}) async-start(bf16[4,4,32,2048]{3,2,1,0:T(8,128)(2,1)} %broadcast_select_fusion), calls=%async_computation.1 | async-start | bytes 4194304 | tf_op jit(solution)/shard_map/all_to_all | solution.py:224
  27.9 509.0 %reduce-scatter.2.cloned.1.call-start = ((), (), s32[]{:S(2)}) async-start(), calls=%async_computation.3 | async-start | bytes 2359296 | tf_op jit(solution)/shard_map/reduce_scatter | solution.py:200
  31.4 3.1 copy-start.4
  87.9 95.6 %collective-permute-start.3 = (bf16[4,128,2048]{2,1,0:T(8,128)(2,1)}, bf16[4,128,2048]{2,1,0:T(8,128)(2,1)}, u32[]{:S(2)}, u32[]{:S(2)}) collective-permute-start(bf16[4,128,2048]{2,1,0:T(8,128)(2,1)} %collective-permute-done.1), channel_id=1, source_target_pairs={{0,1},{1,2},{2,3},{3,4},{4,5},{5,6},{6,7},{7,0},{8,9},{9,10},{10,1... | collective-permute-start | bytes 6291464 | tf_op jit(solution)/shard_map/ppermute | solution.py:29
  170.8 3.6 copy-start.7
  174.4 2.0 copy-start.3
  174.4 3.2 copy-start.5
  175.5 4.0 copy-start.13
  180.6 78.6 %collective-permute-start.2 = (bf16[4,128,2048]{2,1,0:T(8,128)(2,1)}, bf16[4,128,2048]{2,1,0:T(8,128)(2,1)}, u32[]{:S(2)}, u32[]{:S(2)}) collective-permute-start(bf16[4,128,2048]{2,1,0:T(8,128)(2,1)} %collective-permute-done), channel_id=1, source_target_pairs={{0,7},{1,0},{2,1},{3,2},{4,3},{5,4},{6,5},{7,6},{8,15},{9,8},{10,9... | collective-permute-start | bytes 6291464 | tf_op jit(solution)/shard_map/ppermute | solution.py:31
  183.5 113.8 %collective-permute-start.5 = (bf16[4,128,2048]{2,1,0:T(8,128)(2,1)}, bf16[4,128,2048]{2,1,0:T(8,128)(2,1)}, u32[]{:S(2)}, u32[]{:S(2)}) collective-permute-start(bf16[4,128,2048]{2,1,0:T(8,128)(2,1)} %collective-permute-done.3), channel_id=1, source_target_pairs={{0,1},{1,2},{2,3},{3,4},{4,5},{5,6},{6,7},{7,0},{8,9},{9,10},{10,1... | collective-permute-start | bytes 6291464 | tf_op jit(solution)/shard_map/ppermute | solution.py:29
  259.3 222.6 %collective-permute-start.4 = (bf16[4,128,2048]{2,1,0:T(8,128)(2,1)}, bf16[4,128,2048]{2,1,0:T(8,128)(2,1)}, u32[]{:S(2)}, u32[]{:S(2)}) collective-permute-start(bf16[4,128,2048]{2,1,0:T(8,128)(2,1)} %collective-permute-done.2), channel_id=1, source_target_pairs={{0,7},{1,0},{2,1},{3,2},{4,3},{5,4},{6,5},{7,6},{8,15},{9,8},{10,9... | collective-permute-start | bytes 6291464 | tf_op jit(solution)/shard_map/ppermute | solution.py:31
  297.3 189.0 %collective-permute-start.6 = (bf16[4,128,2048]{2,1,0:T(8,128)(2,1)}, bf16[4,128,2048]{2,1,0:T(8,128)(2,1)}, u32[]{:S(2)}, u32[]{:S(2)}) collective-permute-start(bf16[4,128,2048]{2,1,0:T(8,128)(2,1)} %collective-permute-done.5), channel_id=1, source_target_pairs={{0,1},{1,2},{2,3},{3,4},{4,5},{5,6},{6,7},{7,0},{8,9},{9,10},{10,1... | collective-permute-start | bytes 6291464 | tf_op jit(solution)/shard_map/ppermute | solution.py:29
  498.7 4.1 copy-start.16
  498.7 4.1 copy-start.14
  498.7 29.2 %all-to-all-start.1 = ((bf16[4,4,32,2048]{3,2,1,0:T(8,128)(2,1)}), bf16[4,4,32,2048]{3,2,1,0:T(8,128)(2,1)S(1)}, u32[]{:S(2)}, u32[]{:S(2)}) async-start(bf16[4,4,32,2048]{3,2,1,0:T(8,128)(2,1)} %copy.119), calls=%async_computation.2 | async-start | bytes 4194304 | tf_op jit(solution)/shard_map/all_to_all | solution.py:241
  527.9 9.0 %copy-start.1 = (bf16[256,2048]{1,0:T(8,128)(2,1)S(1)}, bf16[256,2048]{1,0:T(8,128)(2,1)}, u32[]{:S(2)}) copy-start(bf16[256,2048]{1,0:T(8,128)(2,1)} %param.27) | copy-start | bytes 3145732
Sparse Core Ops, SparseCore 0:
  9.6 225.9 all-gather.6
  237.3 214.6 all-gather.4
  454.8 36.1 reduce-scatter.1
